TPU v7x, 256 devices: a 4x2x16 block of a 4x16x16 slice. The times are simulated.
256 devices in a mesh: grp: 2 (over y), sp: 32 (over z, core), tp: 4 (over x).
Axes of the slice: x: 4, y: 2, z: 16, core: 2. Of those that a mesh axis runs over, the one named last changes fastest.
The devices are a block of a 4x16x16 slice.
Arguments:
- residual_in: bfloat16 [16384, 2048], P(('grp', 'sp', 'tp')), parts along dimension 0, may hold values from -6 to 6
- query_rows: bfloat16 [16384, 2048], P(('grp', 'sp'), 'tp'), parts along dimension 0, may hold values from -6 to 6
- key_rows: bfloat16 [16384, 512], P(('grp', 'sp'), 'tp'), parts along dimension 0, may hold values from -6 to 6
- value_rows: bfloat16 [16384, 512], P(('grp', 'sp'), 'tp'), parts along dimension 0, may hold values from -6 to 6
- forget_cumsum: float32 [16384, 16], P(('grp', 'sp'), 'tp'), parts along dimension 0, as said below
- head_gain: float32 [2048], P('tp'), may hold values from 0.1 to 1.9
- w_out: bfloat16 [2048, 2048], P('tp'), may hold values from -0.125 to 0.125
- w_up: bfloat16 [2048, 8192], P('sp', 'tp'), may hold values from -0.125 to 0.125
- w_down: bfloat16 [8192, 2048], P('tp', 'sp'), may hold values from -0.0625 to 0.0625
- mixer_gain: float32 [2048], replicated, may hold values from 0.1 to 1.9
- channel_gain: float32 [2048], replicated, may hold values from 0.1 to 1.9
Outputs:
- layer_out: bfloat16 [16384, 2048], P(('grp', 'sp', 'tp')), parts along dimension 0
There are 2 independent parts, one for each index of `grp`. A program takes and returns all parts, laid end to end along the dimension named above; an argument that names none is the same for every part. Nothing has to cross between parts.
Inputs may be any that keep to these rules, and one draw needn't show every extreme that they name: `forget_cumsum`: Non-positive; along the positions, each head's entries never rise.
All inputs are finite; a program needn't handle non-finite values.
Results may differ from a plain program's by a relative error of at most 0.015.
Values may be sent and summed in bfloat16 or wider, within the bound.
A program may use at most 128 MiB of HBM per device.

v0:
```python
import jax
import jax.numpy as jnp
from jax import lax
from jax.sharding import PartitionSpec as P

HD = 128


ALPHA = 8.0**0.25
EPSILON = 1e-05
NEG_FILL = -1e30


def sent_to_all(shard, axis):
    copies = jnp.broadcast_to(shard, (lax.axis_size(axis), *shard.shape))
    return lax.all_to_all(copies, axis, split_axis=0, concat_axis=0, tiled=True)


def joined_along(parts, dim):
    parts = jnp.moveaxis(parts, 0, dim)
    lengths = parts.shape
    return parts.reshape(*lengths[:dim], lengths[dim] * lengths[dim + 1], *lengths[dim + 2 :])


def gather_directly(shard, axis, dim):
    parts = sent_to_all(shard, axis)
    return joined_along(parts, dim)


def sent_together(arrays, axis, dim, along):
    ends, at = ([], 0)
    for a in arrays[:-1]:
        at += a.shape[along]
        ends.append(at)
    both = jnp.concatenate(arrays, axis=along)
    return tuple(jnp.split(lax.all_gather(both, axis, axis=dim, tiled=True), ends, axis=along))


def split_up(shard, dim, size):
    lengths = shard.shape
    parts = shard.reshape(*lengths[:dim], size, lengths[dim] // size, *lengths[dim + 1 :])
    return jnp.moveaxis(parts, dim, 0)


def sum_at_owner(shard, axis, dim):
    parts = split_up(shard, dim, lax.axis_size(axis))
    arrived = lax.all_to_all(parts, axis, split_axis=0, concat_axis=0, tiled=True)
    return arrived.astype(jnp.float32).sum(axis=0)


def rows_first(arrays, axis, dims):
    turned = [jnp.moveaxis(a, dim, 0) for a, dim in zip(arrays, dims)]
    both = jnp.concatenate([t.reshape(len(t), -1) for t in turned], axis=1)
    result, at, finished = (lax.all_gather(both, axis, axis=0, tiled=True), 0, [])
    for t, dim in zip(turned, dims):
        slab = result[:, at : at + t[0].size].reshape(-1, *t.shape[1:])
        finished.append(jnp.moveaxis(slab, 0, dim))
        at += t[0].size
    return tuple(finished)


def layer_scale(inputs, gain_vec):
    centered = inputs - jnp.mean(inputs, axis=-1, keepdims=True)
    variance = jnp.mean(centered * centered, axis=-1, keepdims=True)
    return centered * lax.rsqrt(variance + EPSILON) * gain_vec


def shards(
    residual_in,
    query_rows,
    key_rows,
    value_rows,
    forget_cumsum,
    head_gain,
    w_out,
    w_up,
    w_down,
    mixer_gain,
    channel_gain,
):
    tok_rows = query_rows.shape[0]
    heads_here = forget_cumsum.shape[1]
    kv_here = key_rows.shape[1] // HD
    group_size = heads_here // kv_here
    score_scale = HD ** (-0.5)
    seq_index = lax.axis_index("sp")
    gate_all = gather_directly(forget_cumsum, "sp", 0)
    query_grid = query_rows.reshape(tok_rows, kv_here, group_size, HD)
    query_pos = seq_index * tok_rows + jnp.arange(tok_rows, dtype=jnp.int32)
    last_query = seq_index * tok_rows + tok_rows - 1
    gate_query = forget_cumsum.reshape(tok_rows, kv_here, group_size).transpose(1, 2, 0)

    def attend(carry_state, key_block, value_block, first_row):
        row_count = key_block.shape[0]

        def attend_live(live_state):
            peak_score, denom_sum, accum = live_state
            key_grid = key_block.reshape(row_count, kv_here, HD)
            value_grid = value_block.reshape(row_count, kv_here, HD)
            gate_block = lax.dynamic_slice_in_dim(gate_all, first_row, row_count, 0)
            gate_block = gate_block.reshape(row_count, kv_here, group_size).transpose(1, 2, 0)
            scores = (
                jnp.einsum(
                    "tkgd,ukd->kgtu", query_grid, key_grid, preferred_element_type=jnp.float32
                )
                * score_scale
            )
            scores = scores + gate_query[..., None] - gate_block[:, :, None, :]
            key_pos = first_row + jnp.arange(row_count, dtype=jnp.int32)
            allowed = key_pos[None, :] <= query_pos[:, None]
            scores = jnp.where(allowed, scores, NEG_FILL)
            new_peak = jnp.maximum(peak_score, jnp.max(scores, axis=-1))
            weights = jnp.where(allowed, jnp.exp(scores - new_peak[..., None]), 0.0)
            fade_factor = jnp.exp(peak_score - new_peak)
            denom_sum = denom_sum * fade_factor + jnp.sum(weights, axis=-1)
            accum = accum * fade_factor[..., None] + jnp.einsum(
                "kgtu,ukd->kgtd",
                weights.astype(jnp.bfloat16),
                value_grid,
                preferred_element_type=jnp.float32,
            )
            return (new_peak, denom_sum, accum)

        return lax.cond(
            first_row <= last_query, attend_live, lambda kept_state: kept_state, carry_state
        )

    fold_init = (
        jnp.full((kv_here, group_size, tok_rows), NEG_FILL, jnp.float32),
        jnp.zeros((kv_here, group_size, tok_rows), jnp.float32),
        jnp.zeros((kv_here, group_size, tok_rows, HD), jnp.float32),
    )
    carry_state = fold_init
    key_piece, value_piece = sent_together((key_rows, value_rows), "sp", 0, 1)
    row_count = key_piece.shape[0]
    block_span = 1024

    def scan_block(scan_state, block_index):
        offset = block_index * block_span
        next_state = attend(
            scan_state,
            lax.dynamic_slice_in_dim(key_piece, offset, block_span, 0),
            lax.dynamic_slice_in_dim(value_piece, offset, block_span, 0),
            offset,
        )
        return (next_state, None)

    carry_state, unused = lax.scan(
        scan_block, carry_state, jnp.arange(row_count // block_span, dtype=jnp.int32)
    )
    peak_score, denom_sum, accum = carry_state
    attended = accum / denom_sum[..., None]
    normed = attended * lax.rsqrt(jnp.mean(attended * attended, axis=-1, keepdims=True) + EPSILON)
    normed = normed * head_gain.reshape(kv_here, group_size, 1, HD)
    heads_out = normed.transpose(2, 0, 1, 3).reshape(tok_rows, heads_here * HD).astype(jnp.bfloat16)
    branch = sum_at_owner(
        jnp.dot(heads_out, w_out, preferred_element_type=jnp.float32).astype(jnp.bfloat16), "tp", 0
    )
    mid_rows = layer_scale(ALPHA * residual_in.astype(jnp.float32) + branch, mixer_gain).astype(
        jnp.bfloat16
    )
    mid_all = gather_directly(mid_rows, "tp", 0)
    up_full, down_full = rows_first((w_up, w_down), "sp", (0, 1))
    lifted = jnp.dot(mid_all, up_full, preferred_element_type=jnp.float32)
    active = jnp.square(jax.nn.relu(lifted)).astype(jnp.bfloat16)
    lowered = sum_at_owner(
        jnp.dot(active, down_full, preferred_element_type=jnp.float32).astype(jnp.bfloat16), "tp", 0
    )
    return layer_scale(ALPHA * mid_rows.astype(jnp.float32) + lowered, channel_gain).astype(
        jnp.bfloat16
    )


def solution(mesh):
    placed = (
        P(("grp", "sp", "tp"), None),
        P(("grp", "sp"), "tp"),
        P(("grp", "sp"), "tp"),
        P(("grp", "sp"), "tp"),
        P(("grp", "sp"), "tp"),
        P("tp"),
        P("tp", None),
        P("sp", "tp"),
        P("tp", "sp"),
        P(),
        P(),
    )
    return jax.shard_map(
        shards, mesh=mesh, in_specs=placed, out_specs=P(("grp", "sp", "tp"), None), check_vma=False
    )
```

profile of v0, /device:TPU:33, one launch (start us, length us, event | category | flops | bytes accessed | tf_op | source)
XLA Modules:
  0.0 240.7 jit_solution(6481389775492686533)
XLA Ops:
  6.5 0.0 copy-start
  6.6 0.0 all-gather.3.cloned.1.call-start
  6.6 1.7 pad_maximum_fusion.1
  8.2 0.1 all-gather.3.cloned.1.call-update
  8.3 0.1 all-gather.5.cloned.1.call-start
  8.4 1.9 pad_maximum_fusion
  10.3 0.1 all-gather.5.cloned.1.call-update
  10.4 1.4 broadcast_in_dim.53
  11.7 25.5 %all-to-all-start = ((f32[32,256,4]{1,2,0:T(4,128)}), f32[32,256,4]{1,2,0:T(4,128)S(1)}, u32[]{:S(2)}, u32[]{:S(2)}) async-start(f32[32,256,4]{1,2,0:T(4,128)} %broadcast_in_dim.53), calls=%async_computation | async-start | bytes 262144 | tf_op jit(solution)/shard_map/all_to_all | solution.py:16
  37.2 1.1 copy.18
  38.3 0.2 copy.19
  38.5 0.0 copy-start.2
  38.5 60.4 %all-gather.3.cloned.1.call-done = bf16[8192,256]{1,0:T(8,128)(2,1)} async-done(((bf16[256,256]{1,0:T(8,128)(2,1)}), bf16[8192,256]{1,0:T(8,128)(2,1)}) %all-gather.3.cloned.1.call-update) | async-done | bytes 4194320 | tf_op jit(solution)/shard_map/all_gather | solution.py:36
  98.9 4.5 %fusion.51 = (bf16[8192,128]{1,0:T(8,128)(2,1)}, bf16[8192,128]{1,0:T(8,128)(2,1)}) fusion(bf16[8192,256]{1,0:T(8,128)(2,1)} %all-gather.3.cloned.1.call-done), kind=kLoop, calls=%fused_computation.63 | loop fusion | bytes 8388608 | tf_op jit(solution)/shard_map/split | solution.py:36
  103.3 0.0 all-to-all-done
  103.4 0.0 copy-done.2
  103.4 0.0 copy-start.5
  103.4 17.7 %while.15 = (s32[]{:T(128)}, f32[1,4,256]{2,1,0:T(4,128)S(1)}, f32[1,4,256]{2,1,0:T(4,128)S(1)}, f32[1,4,256,128]{3,2,1,0:T(8,128)S(1)}, s32[8]{0:T(128)S(1)}, /...) while((s32[]{:T(128)}, f32[1,4,256]{2,1,0:T(4,128)S(1)}, ...), condition=%wide.region_5.6_spmd.clone, body=%wide.region_0.5_spmd.clone.sunk | while | flops 557322496 | bytes 15638897 | solution.py:148
  103.5 0.6 dynamic_slice.41
  104.7 7.4 %conditional.3 = ((f32[1,4,256]{2,1,0:T(4,128)S(1)}, f32[1,4,256]{2,1,0:T(4,128)S(1)}, f32[1,4,256,128]{3,2,1,0:T(8,128)S(1)})) conditional(s32[]{:T(128)} %convert_element_type.91, (f32[1,4,256]{2,1,0:T(4,128)S(1)}, f32[1,4,256]{2,1,0:T(4,128)S(1)}, f32[1,4,256,128]{3,2,1,0:T(8,128)S(1)}) %tuple.46, (s32[]{:T(128)}, s32[]{:T(128)}, ...), branch_computations={%region_1.1_spmd, %region_2.4_spmd} | conditional | flops 557322496 | bytes 15637590 | solution.py:124
  104.7 0.1 dynamic-slice_bitcast_fusion
  104.8 0.2 broadcast_compare_fusion
  105.0 2.2 fusion.6
  107.3 3.3 %fusion.14 = f32[1,4,256,128]{3,2,1,0:T(8,128)S(1)} fusion(f32[1024,256,4]{1,0,2:T(8,128)S(1)} %get-tuple-element.279, f32[4,256]{1,0:T(4,128)S(1)} %bitcast.81, f32[4,1024]{1,0:T(4,128)S(1)} %dynamic-slice_bitcast_fusion, f32[4,256]{1,0:T(4,128)S(1)} %bitcast.93, pred[256,1024]{0,1:T(8,128)(4,1)S(1)} %broadcast_compare_fusion, ...), kind=kOutput, calls=%fused_computation.12 | convolution fusion | flops 276037632 | bytes 5795844 | tf_op jit(solution)/shard_map/while/body/eval_jaxpr/cond/branch_1_fun/kgtu,ukd->kgtd/dot_general | solution.py:116
  110.6 1.5 fusion.5
  112.1 0.6 dynamic_slice.41
  113.4 0.6 dynamic_slice.41
  114.7 0.6 dynamic_slice.41
  116.0 0.6 dynamic_slice.41
  117.3 0.6 dynamic_slice.41
  118.6 0.6 dynamic_slice.41
  119.9 0.6 dynamic_slice.41
  121.2 0.2 copy.20
  121.4 0.0 copy-start.1
  121.4 0.1 multiply_reduce_fusion.2
  121.5 0.0 copy-done.5
  121.5 0.1 multiply_convert_fusion.2
  121.6 0.0 copy-done
  121.6 0.0 copy-start.3
  121.7 0.7 convolution_convert_fusion
  122.4 18.6 %all_to_all.20 = bf16[4,64,2048]{2,1,0:T(8,128)(2,1)S(1)} all-to-all(bf16[4,64,2048]{2,1,0:T(8,128)(2,1)S(1)} %bitcast.80), channel_id=1, replica_groups=mesh['grp'=2,'sp'=32,'tp'=4] {'tp'}, dimensions={0} | all-to-all | bytes 2097152 | tf_op jit(solution)/shard_map/all_to_all | solution.py:47
  141.0 0.2 convert_reduce_fusion.1
  141.2 0.0 copy-done.1
  141.2 0.2 fusion.48
  141.4 0.2 multiply_reduce_fusion.1
  141.6 0.0 copy-done.3
  141.6 0.1 multiply_convert_fusion.1
  141.7 0.1 broadcast_in_dim.54
  141.9 16.0 %all_to_all.21 = bf16[4,64,2048]{2,1,0:T(8,128)(2,1)S(1)} all-to-all(bf16[4,64,2048]{2,1,0:T(8,128)(2,1)S(1)} %broadcast_in_dim.54), channel_id=1, replica_groups=mesh['grp'=2,'sp'=32,'tp'=4] {'tp'}, dimensions={0} | all-to-all | bytes 2097152 | tf_op jit(solution)/shard_map/all_to_all | solution.py:16
  157.8 44.6 %all-gather.5.cloned.1.call-done = bf16[2048,4096]{1,0:T(8,128)(2,1)} async-done(((bf16[64,4096]{1,0:T(8,128)(2,1)}), bf16[2048,4096]{1,0:T(8,128)(2,1)}) %all-gather.5.cloned.1.call-update) | async-done | bytes 16777232 | tf_op jit(solution)/shard_map/all_gather | solution.py:54
  202.4 11.3 %fusion.42 = bf16[256,2048]{1,0:T(8,128)(2,1)} fusion(bf16[2048,4096]{1,0:T(8,128)(2,1)} %all-gather.5.cloned.1.call-done, bf16[256,2048]{1,0:T(8,128)(2,1)S(1)} %bitcast.83), kind=kOutput, calls=%fused_computation.40 | convolution fusion | flops 4297064448 | bytes 18874368 | tf_op jit(solution)/shard_map/dot_general | solution.py:167
  213.7 0.0 copy-start.4
  213.7 18.7 %all_to_all.22 = bf16[4,64,2048]{2,1,0:T(8,128)(2,1)S(1)} all-to-all(bf16[4,64,2048]{2,1,0:T(8,128)(2,1)} %bitcast.84), channel_id=1, replica_groups=mesh['grp'=2,'sp'=32,'tp'=4] {'tp'}, dimensions={0} | all-to-all | bytes 2097152 | tf_op jit(solution)/shard_map/all_to_all | solution.py:47
  232.4 0.2 convert_reduce_fusion
  232.6 0.2 fusion.49
  232.8 0.2 multiply_reduce_fusion
  233.0 0.0 copy-done.4
  233.0 0.8 multiply_convert_fusion
  (29 shorter events, 0.2 us)
Async XLA Ops:
  6.5 115.1 %copy-start = (bf16[512,2048]{1,0:T(8,128)(2,1)S(1)}, bf16[512,2048]{1,0:T(8,128)(2,1)}, u32[]{:S(2)}) copy-start(bf16[512,2048]{1,0:T(8,128)(2,1)} %param.21) | copy-start | bytes 6291460
  6.6 92.3 %all-gather.3.cloned.1.call-start = ((), (), s32[]{:S(2)}) async-start(), calls=%async_computation.4 | async-start | bytes 4325376 | tf_op jit(solution)/shard_map/all_gather | solution.py:36
  8.3 194.1 %all-gather.5.cloned.1.call-start = ((), (), s32[]{:S(2)}) async-start(), calls=%async_computation.5 | async-start | bytes 17301504 | tf_op jit(solution)/shard_map/all_gather | solution.py:54
  11.7 91.6 %all-to-all-start = ((f32[32,256,4]{1,2,0:T(4,128)}), f32[32,256,4]{1,2,0:T(4,128)S(1)}, u32[]{:S(2)}, u32[]{:S(2)}) async-start(f32[32,256,4]{1,2,0:T(4,128)} %broadcast_in_dim.53), calls=%async_computation | async-start | bytes 262144 | tf_op jit(solution)/shard_map/all_to_all | solution.py:16
  38.5 64.9 %copy-start.2 = (f32[256,4]{0,1:T(4,128)S(1)}, f32[256,4]{0,1:T(4,128)}, u32[]{:S(2)}) copy-start(f32[256,4]{0,1:T(4,128)} %param.19) | copy-start | bytes 12292
  103.4 18.1 %copy-start.5 = (f32[512]{0:T(512)S(1)}, f32[512]{0:T(512)}, u32[]{:S(2)}) copy-start(f32[512]{0:T(512)} %param.20) | copy-start | bytes 6148
  121.4 19.8 %copy-start.1 = (bf16[64,2048]{1,0:T(8,128)(2,1)S(1)}, bf16[64,2048]{1,0:T(8,128)(2,1)}, u32[]{:S(2)}) copy-start(bf16[64,2048]{1,0:T(8,128)(2,1)} %param.15) | copy-start | bytes 786436
  121.6 19.9 %copy-start.3 = (f32[2048]{0:T(1024)S(1)}, f32[2048]{0:T(1024)}, u32[]{:S(2)}) copy-start(f32[2048]{0:T(1024)} %param.24) | copy-start | bytes 24580
  213.7 19.3 %copy-start.4 = (f32[2048]{0:T(1024)S(1)}, f32[2048]{0:T(1024)}, u32[]{:S(2)}) copy-start(f32[2048]{0:T(1024)} %param.25) | copy-start | bytes 24580
Sparse Core Ops, SparseCore 0:
  9.2 89.6 all-gather.2
  100.7 101.6 all-gather.4
where the time goes:
time: 242 us; the launch traced here: 241 us
  waiting for transfers between devices  105 us (43%)
  blocking collectives  53.3 us (22%)
  starting transfers between devices  25.5 us (11%)
  matrix products  17.5 us (7%)
  between operations  13.6 us (6%)
  local copies, waits for them, and re-layouts  12.3 us (5%)
  other arithmetic  7.65 us (3%)
  loops' own time  5.7 us (2%)
    all_gather x1, waiting for transfers between devices, sent_together(): lax.all_gather(both, axis, axis=dim, tiled=True)  60.4 us
    all_gather x1, waiting for transfers between devices, rows_first(): lax.all_gather(both, axis, axis=0, tiled=True)  44.6 us
    all_to_all x2, blocking collectives, sum_at_owner(): lax.all_to_all(parts, axis, split_axis=0, concat_axis=0, tiled=True)  37.3 us
    all_to_all x1, starting transfers between devices, sent_to_all(): return lax.all_to_all(copies, axis, split_axis=0, concat_axis=0, tiled=True)  25.5 us
    all_to_all x1, blocking collectives, sent_to_all(): return lax.all_to_all(copies, axis, split_axis=0, concat_axis=0, tiled=True)  16 us
    dot_general x1, matrix products, shards(): jnp.dot(active, down_full, preferred_element_type=jnp.float32)  11.3 us
    another operation x1, loops' own time, shards(): lax.scan(scan_block, carry_state, jnp.arange(row_count // block_span, dty...  5.53 us
  transfers between devices with their start and end apart: 3, of which 2 were waited for; matrix products, arithmetic and copies ran while one was open for 10% of the time, Pallas kernels for 0%

commit v1 on v0

v1 whole, which is shorter than its diff:
```python
import functools

import jax
import jax.numpy as jnp
from jax import lax
from jax.experimental import pallas as pl
from jax.experimental.pallas import tpu as pltpu
from jax.sharding import PartitionSpec as P

HD = 128
ALPHA = 8.0**0.25
EPSILON = 1e-05
NEG_FILL = -1e30
LOG2E = 1.4426950408889634
MESH = pl.DeviceIdType.MESH
F32 = jnp.float32
BF16 = jnp.bfloat16

KV, GATE, UP, DOWN = 0, 1, 2, 3


def dot_nt(a, b):
    return lax.dot_general(a, b, (((1,), (1,)), ((), ())), preferred_element_type=F32)


def dot_nn(a, b):
    return lax.dot_general(a, b, (((1,), (0,)), ((), ())), preferred_element_type=F32)


def layer_kernel(
    chips,
    q_hbm, k_hbm, v_hbm, f_hbm, res_ref, hgain_ref, wo_hbm, wu_hbm, wd_hbm, mgain_ref, cgain_ref,
    out_ref,
    q_s, kv, gate, wo_s, wu, wd_raw, wd, acc, m_s, l_s, heads, bp, b1, b2t, b2, mid, act,
    dp, d1, d2t, d2, d3t, d3, keep, low,
    ring_send, ring_recv, twin_send, twin_recv, local, bx_send, bx_recv, mx_send, mx_recv,
    dx_send, dx_recv,
):
    far = chips // 2
    grp, sp, tp = lax.axis_index("grp"), lax.axis_index("sp"), lax.axis_index("tp")
    z, core = sp // 2, sp % 2
    pair = grp % 2
    rows = q_s.shape[1]
    ffh = act.shape[1]
    right = (grp, ((z + 1) % chips) * 2 + core, tp)
    left = (grp, ((z + chips - 1) % chips) * 2 + core, tp)
    twin = (grp, z * 2 + 1 - core, tp)
    xa = tp + 1 - 2 * (tp % 2)
    xb = 3 - tp
    dev_a, dev_b = (grp, sp, xa), (grp, sp, xb)
    dev_y = (grp + 1 - 2 * pair, sp, tp)
    peers = (right, left, twin, dev_a, dev_b, dev_y)
    bufs = (kv, gate, wu, wd)

    def remote(src, dst, ss, rs, dev):
        return pltpu.make_async_remote_copy(
            src_ref=src, dst_ref=dst, send_sem=ss, recv_sem=rs, device_id=dev, device_id_type=MESH
        )

    def when(cond, fn):
        if isinstance(cond, bool):
            if cond:
                fn()
        else:
            pl.when(cond)(fn)

    def both(a, b):
        return (a and b) if isinstance(a, bool) and isinstance(b, bool) else jnp.logical_and(a, b)

    def ring_copy(st, way, slot, s):
        buf = bufs[st].at[slot]
        return remote(buf, buf, ring_send.at[st, way], ring_recv.at[st, way, s], right if way == 0 else left)

    def twin_copy(st, way, slot, s):
        buf = bufs[st].at[slot]
        return remote(buf, buf, twin_send.at[st, way], twin_recv.at[st, way, s], twin)

    def chip_at(way, s):
        return (z + chips - s) % chips if way == 0 else (z + s) % chips

    def ring_begin(st):
        ring_copy(st, 0, sp, 1).start()
        ring_copy(st, 1, sp, 1).start()
        twin_copy(st, 0, sp, 0).start()

    def ring_step(st, s):
        def one(way, last):
            slot = chip_at(way, s) * 2 + core
            ring_copy(st, way, slot, s).wait_recv()
            ring_copy(st, way, slot, s).wait_send()

            when(s < last, lambda: ring_copy(st, way, slot, s + 1).start())
            when(way == 0 or s > 1, lambda: twin_copy(st, way, slot, s).wait_send())
            twin_copy(st, way, slot, s).start()

        one(0, far)
        when(s < far, lambda: one(1, far - 1))

    def twin_wait(st, s):
        twin_copy(st, 0, chip_at(0, s) * 2 + 1 - core, s).wait_recv()
        when(
            both(s > 0, s < far),
            lambda: twin_copy(st, 1, chip_at(1, s) * 2 + 1 - core, s).wait_recv(),
        )

    def ring_end(st):
        twin_copy(st, 0, sp, 0).wait_send()
        twin_copy(st, 1, sp, 0).wait_send()

    loads = [
        pltpu.make_async_copy(k_hbm, kv.at[sp, 0], local.at[0]),
        pltpu.make_async_copy(v_hbm, kv.at[sp, 1], local.at[1]),
        pltpu.make_async_copy(f_hbm, gate.at[sp], local.at[2]),
        pltpu.make_async_copy(wu_hbm.at[:, pl.ds(pl.multiple_of(pair * ffh, ffh), ffh)], wu.at[sp], local.at[3]),
        pltpu.make_async_copy(wd_hbm.at[pl.ds(pl.multiple_of(pair * ffh, ffh), ffh)], wd_raw, local.at[4]),
        pltpu.make_async_copy(wo_hbm, wo_s, local.at[5]),
    ]
    loads += [pltpu.make_async_copy(q_hbm.at[:, pl.ds(h * HD, HD)], q_s.at[h], local.at[6 + h]) for h in range(4)]
    for c in loads:
        c.start()

    barrier = pltpu.get_barrier_semaphore()
    for dev in peers:
        pl.semaphore_signal(barrier, inc=1, device_id=dev, device_id_type=MESH)
    pl.semaphore_wait(barrier, len(peers))

    for c in loads[:3]:
        c.wait()
    ring_begin(KV)
    ring_begin(GATE)

    gate_base = [None] * 4
    own_gate = gate[sp]
    for h in range(4):
        gate_base[h] = own_gate[h : h + 1, 0:1]

    def scores(h, src):
        s = dot_nt(q_s[h], kv[src, 0])
        bias = (gate_base[h] - gate[src][h : h + 1, :]) * LOG2E
        return s * (HD**-0.5 * LOG2E) + bias

    def spread(col):
        return jnp.broadcast_to(col, (rows, HD))

    for c in loads[6:]:
        c.wait()
    causal = lax.broadcasted_iota(jnp.int32, (rows, rows), 1) <= lax.broadcasted_iota(jnp.int32, (rows, rows), 0)
    for h in range(4):
        s = jnp.where(causal, scores(h, sp), NEG_FILL)
        m = spread(jnp.max(s, axis=1, keepdims=True))
        p = jnp.exp2(s - jnp.concatenate([m] * (rows // HD), axis=1))
        m_s[h] = m
        l_s[h] = spread(jnp.sum(p, axis=1, keepdims=True))
        acc[h] = dot_nn(p.astype(BF16), kv[sp, 1])

    def attend(srcs):
        for h in range(4):
            ss = [scores(h, src) for src in srcs]
            top = functools.reduce(jnp.maximum, ss)
            m_old = m_s[h]
            m = jnp.maximum(m_old, spread(jnp.max(top, axis=1, keepdims=True)))
            wide = jnp.concatenate([m] * (rows // HD), axis=1)
            ps = [jnp.exp2(s - wide) for s in ss]
            fade = jnp.exp2(m_old - m)
            total = functools.reduce(jnp.add, ps)
            m_s[h] = m
            l_s[h] = l_s[h] * fade + spread(jnp.sum(total, axis=1, keepdims=True))
            out = dot_nn(ps[0].astype(BF16), kv[srcs[0], 1])
            for p, src in zip(ps[1:], srcs[1:]):
                out = out + dot_nn(p.astype(BF16), kv[src, 1])
            acc[h] = acc[h] * fade + out

    def attend_step(s):
        @pl.when(z - s >= 0)
        def _():
            c = chip_at(0, s) * 2
            attend([c, c + 1])

        @pl.when(both(s < far, z + s >= chips) if not isinstance(s, int) else jnp.logical_and(z + s >= chips, s < far))
        def _():
            c = chip_at(1, s) * 2
            attend([c, c + 1])

    def kv_step(s, carry):
        ring_step(KV, s)
        ring_step(GATE, s)
        twin_wait(KV, s - 1)
        twin_wait(GATE, s - 1)

        @pl.when(jnp.logical_and(s == 1, core == 1))
        def _():
            attend([sp - 1])

        @pl.when(s > 1)
        def _():
            attend_step(s - 1)

        return carry

    lax.fori_loop(1, far + 1, kv_step, 0)
    loads[3].wait()
    ring_begin(UP)
    twin_wait(KV, far)
    twin_wait(GATE, far)
    attend_step(far)
    ring_end(KV)
    ring_end(GATE)

    loads[4].wait()
    cols = wd_raw.shape[1]
    eye = (
        lax.broadcasted_iota(jnp.int32, (cols, cols), 0) == lax.broadcasted_iota(jnp.int32, (cols, cols), 1)
    ).astype(BF16)
    wd[sp] = dot_nt(eye, wd_raw[...]).astype(BF16)

    loads[5].wait()
    for h in range(4):
        att = acc[h] / l_s[h]
        norm = lax.rsqrt(jnp.mean(att * att, axis=1, keepdims=True) + EPSILON)
        heads[:, h * HD : (h + 1) * HD] = (att * norm * hgain_ref[h : h + 1, :]).astype(BF16)
    half = bp.shape[3]
    own = bp.shape[2]
    for j in range(4):
        w = half // 2
        part = dot_nn(heads[...], wo_s[:, j * w : (j + 1) * w]).astype(BF16)
        bp[j // 2, :, :, (j % 2) * w : (j % 2 + 1) * w] = part.reshape(4, own, w)

    far_a = 3 - xa
    first = (dev_a, dev_b)
    second = (dev_b, dev_a)
    first_x = (xa, xb)
    second_x = (xb, xa)

    def b1_copy(hf, j):
        src = bp.at[hf, first_x[hf] if j == 0 else far_a]
        return remote(src, b1.at[hf, j], bx_send.at[hf, j], bx_recv.at[hf, j], first[hf])

    def b2_copy(hf):
        return remote(b2t.at[hf], b2.at[hf], bx_send.at[hf, 2], bx_recv.at[hf, 2], second[hf])

    for hf in range(2):
        b1_copy(hf, 1).start()
    for hf in range(2):
        b1_copy(hf, 0).start()
    ring_step(UP, 1)
    for hf in range(2):
        b1_copy(hf, 1).wait_recv()
        b2t[hf] = (bp[hf, second_x[hf]].astype(F32) + b1[hf, 1].astype(F32)).astype(BF16)
        b2_copy(hf).start()
    ring_step(UP, 2)
    sums = []
    for hf in range(2):
        b1_copy(hf, 0).wait_recv()
    ring_step(UP, 3)
    for hf in range(2):
        b2_copy(hf).wait_recv()
        part = bp[hf, tp].astype(F32) + b1[hf, 0].astype(F32) + b2[hf].astype(F32)
        sums.append(ALPHA * res_ref[:, hf * half : (hf + 1) * half].astype(F32) + part)

    def layer_norm(parts, gain_ref):
        width = 2 * half
        mean = sum(jnp.sum(p, axis=1, keepdims=True) for p in parts) * (1.0 / width)
        parts = [p - mean for p in parts]
        var = sum(jnp.sum(p * p, axis=1, keepdims=True) for p in parts) * (1.0 / width)
        inv = lax.rsqrt(var + EPSILON)
        return [
            (p * inv * gain_ref[:, i * half : (i + 1) * half]).astype(BF16) for i, p in enumerate(parts)
        ]

    for hf, part in enumerate(layer_norm(sums, mgain_ref)):
        mid[hf, tp, pair] = part

    def my_copy(hf):
        return remote(mid.at[hf, tp, pair], mid.at[hf, tp, pair], mx_send.at[hf, 0], mx_recv.at[hf, 0], dev_y)

    def m1_copy(hf, j):
        ref = mid.at[hf, tp, pair if j == 0 else 1 - pair]
        return remote(ref, ref, mx_send.at[hf, 1 + j], mx_recv.at[hf, 1 + j], first[hf])

    def m2_copy(hf, j):
        ref = mid.at[hf, tp if j == 0 else first_x[hf]]
        return remote(ref, ref, mx_send.at[hf, 3 + j], mx_recv.at[hf, 3 + j], second[hf])

    for hf in range(2):
        my_copy(hf).start()
        m1_copy(hf, 0).start()
    ring_step(UP, 4)
    for hf in range(2):
        my_copy(hf).wait_recv()
        m1_copy(hf, 1).start()
        m2_copy(hf, 0).start()
    ring_step(UP, 5)
    ring_step(UP, 6)
    for hf in range(2):
        m1_copy(hf, 0).wait_recv()
        m1_copy(hf, 1).wait_recv()
        m2_copy(hf, 1).start()
    ring_step(UP, 7)
    ring_step(UP, 8)
    ring_begin(DOWN)
    for s in range(far + 1):
        twin_wait(UP, s)
    ring_step(DOWN, 1)
    ring_step(DOWN, 2)
    for hf in range(2):
        m2_copy(hf, 0).wait_recv()
        m2_copy(hf, 1).wait_recv()
    ring_end(UP)

    toks = act.shape[0]
    tile = 256

    def up_tile(j, carry):
        cs = pl.ds(pl.multiple_of(j * tile, tile), tile)
        total = None
        for hf in range(2):
            blocks = wu.shape[0] // 2
            w = wu[hf * blocks : (hf + 1) * blocks, :, cs].reshape(half, tile)
            part = dot_nn(mid[hf].reshape(toks, half), w)
            total = part if total is None else total + part
        pos = jnp.maximum(total, 0.0)
        act[:, cs] = (pos * pos).astype(BF16)
        return carry

    lax.fori_loop(0, ffh // tile // 2, up_tile, 0)
    ring_step(DOWN, 3)
    lax.fori_loop(ffh // tile // 2, ffh // tile, up_tile, 0)
    early = 3

    wide = 2 * cols

    def chunk_chip(t, hf):
        return jnp.where(t == far, z, chip_at(0, t)) if hf == 0 else jnp.where(t == far, chip_at(0, t), chip_at(1, t))

    def d1_copy(t, hf, j):
        src = dp.at[t - 1, hf, first_x[hf] if j == 0 else far_a]
        return remote(src, d1.at[t - 1, hf, j], dx_send.at[t - 1, hf, j], dx_recv.at[t - 1, hf, j], first[hf])

    def d2_copy(t, hf):
        return remote(
            d2t.at[t - 1, hf], d2.at[t - 1, hf], dx_send.at[t - 1, hf, 2], dx_recv.at[t - 1, hf, 2], second[hf]
        )

    def d3_copy(t, hf):
        return remote(
            d3t.at[t - 1, hf], d3.at[t - 1, hf], dx_send.at[t - 1, hf, 3], dx_recv.at[t - 1, hf, 3], dev_y
        )

    def down_step(i, carry):
        @pl.when(jnp.logical_and(i > early, i <= far))
        def _():
            ring_step(DOWN, i)

        @pl.when(jnp.logical_and(i >= 2, i <= far + 1))
        def _():
            t = i - 1
            twin_wait(DOWN, t)

            @pl.when(t == far)
            def _():
                twin_wait(DOWN, 0)

            w = jnp.concatenate(
                [wd[pl.ds(chunk_chip(t, hf) * 2, 2)].reshape(wide, ffh) for hf in range(2)], axis=0
            )
            part = dot_nt(act[...], w).astype(BF16)
            for hf in range(2):
                dp[t - 1, hf] = part[:, hf * wide : (hf + 1) * wide].reshape(4, 2, own, wide)
                d1_copy(t, hf, 1).start()
                d1_copy(t, hf, 0).start()

        @pl.when(jnp.logical_and(i >= 3, i <= far + 2))
        def _():
            t = i - 2
            for hf in range(2):
                d1_copy(t, hf, 1).wait_recv()
                d2t[t - 1, hf] = (
                    dp[t - 1, hf, second_x[hf]].astype(F32) + d1[t - 1, hf, 1].astype(F32)
                ).astype(BF16)
                d2_copy(t, hf).start()

        @pl.when(jnp.logical_and(i >= 4, i <= far + 3))
        def _():
            t = i - 3
            for hf in range(2):
                d1_copy(t, hf, 0).wait_recv()
                d2_copy(t, hf).wait_recv()

                def whole(y):
                    return (
                        dp[t - 1, hf, tp, y].astype(F32)
                        + d1[t - 1, hf, 0, y].astype(F32)
                        + d2[t - 1, hf, y].astype(F32)
                    )

                d3t[t - 1, hf] = whole(1 - pair).astype(BF16)
                d3_copy(t, hf).start()
                keep[t - 1, hf] = whole(pair)

        @pl.when(i >= 5)
        def _():
            t = i - 4
            for hf in range(2):
                d3_copy(t, hf).wait_recv()
                cs = pl.ds(pl.multiple_of(chunk_chip(t, hf) * wide, wide), wide)
                low[:, cs] = keep[t - 1, hf] + d3[t - 1, hf].astype(F32)
                for j in range(2):
                    d1_copy(t, hf, j).wait_send()
                d2_copy(t, hf).wait_send()
                d3_copy(t, hf).wait_send()

        return carry

    lax.fori_loop(1, far + 5, down_step, 0)
    ring_end(DOWN)

    sums = [
        ALPHA * mid[hf, tp, pair].astype(F32) + low[:, hf * half : (hf + 1) * half] for hf in range(2)
    ]
    for hf, part in enumerate(layer_norm(sums, cgain_ref)):
        out_ref[:, hf * half : (hf + 1) * half] = part

    for hf in range(2):
        for j in range(2):
            b1_copy(hf, j).wait_send()
            m1_copy(hf, j).wait_send()
            m2_copy(hf, j).wait_send()
        b2_copy(hf).wait_send()
        my_copy(hf).wait_send()


def solution(mesh):
    spn, tpn = mesh.shape["sp"], mesh.shape["tp"]
    chips = spn // 2
    assert spn % 4 == 0 and tpn == 4 and mesh.shape["grp"] % 2 == 0

    def shards(res, q, k, v, f, hgain, wo, wu, wd, mgain, cgain):
        rows = q.shape[0]
        own, width = res.shape
        half = width // 2
        up_rows, ff = wu.shape
        ffh = ff // 2
        cols = wd.shape[1]
        wide = 2 * cols
        far = chips // 2
        toks = 2 * 4 * own
        f_t = jnp.pad(f.T, ((0, 4), (0, 0)))
        any_spec = pl.BlockSpec(memory_space=pl.ANY)
        vmem = pl.BlockSpec(memory_space=pltpu.VMEM)
        dma = pltpu.SemaphoreType.DMA
        return pl.pallas_call(
            functools.partial(layer_kernel, chips),
            out_shape=jax.ShapeDtypeStruct((own, width), BF16),
            in_specs=[any_spec, any_spec, any_spec, any_spec, vmem, vmem, any_spec, any_spec, any_spec, vmem, vmem],
            out_specs=vmem,
            scratch_shapes=[
                pltpu.VMEM((4, rows, HD), BF16),
                pltpu.VMEM((spn, 2, rows, HD), BF16),
                pltpu.VMEM((spn, 8, rows), F32),
                pltpu.VMEM(wo.shape, BF16),
                pltpu.VMEM((spn, up_rows, ffh), BF16),
                pltpu.VMEM((ffh, cols), BF16),
                pltpu.VMEM((spn, cols, ffh), BF16),
                pltpu.VMEM((4, rows, HD), F32),
                pltpu.VMEM((4, rows, HD), F32),
                pltpu.VMEM((4, rows, HD), F32),
                pltpu.VMEM((rows, 4 * HD), BF16),
                pltpu.VMEM((2, 4, own, half), BF16),
                pltpu.VMEM((2, 2, own, half), BF16),
                pltpu.VMEM((2, own, half), BF16),
                pltpu.VMEM((2, own, half), BF16),
                pltpu.VMEM((2, 4, 2, own, half), BF16),
                pltpu.VMEM((toks, ffh), BF16),
                pltpu.VMEM((far, 2, 4, 2, own, wide), BF16),
                pltpu.VMEM((far, 2, 2, 2, own, wide), BF16),
                pltpu.VMEM((far, 2, 2, own, wide), BF16),
                pltpu.VMEM((far, 2, 2, own, wide), BF16),
                pltpu.VMEM((far, 2, own, wide), BF16),
                pltpu.VMEM((far, 2, own, wide), BF16),
                pltpu.VMEM((far, 2, own, wide), F32),
                pltpu.VMEM((own, width), F32),
                dma((4, 2)),
                dma((4, 2, far + 1)),
                dma((4, 2)),
                dma((4, 2, far + 1)),
                dma((10,)),
                dma((2, 3)),
                dma((2, 3)),
                dma((2, 5)),
                dma((2, 5)),
                dma((far, 2, 4)),
                dma((far, 2, 4)),
            ],
            compiler_params=pltpu.CompilerParams(
                collective_id=0, has_side_effects=True, vmem_limit_bytes=56 * 1024 * 1024
            ),
            name="layer",
        )(q, k, v, f_t, res, hgain.reshape(4, HD), wo, wu, wd, mgain.reshape(1, width), cgain.reshape(1, width))

    def body(residual_in, query_rows, key_rows, value_rows, forget_cumsum, head_gain, w_out, w_up, w_down, mixer_gain, channel_gain):
        return shards(
            residual_in, query_rows, key_rows, value_rows, forget_cumsum, head_gain, w_out, w_up, w_down,
            mixer_gain, channel_gain,
        )

    placed = (
        P(("grp", "sp", "tp"), None),
        P(("grp", "sp"), "tp"),
        P(("grp", "sp"), "tp"),
        P(("grp", "sp"), "tp"),
        P(("grp", "sp"), "tp"),
        P("tp"),
        P("tp", None),
        P("sp", "tp"),
        P("tp", "sp"),
        P(),
        P(),
    )
    return jax.shard_map(
        body, mesh=mesh, in_specs=placed, out_specs=P(("grp", "sp", "tp"), None), check_vma=False
    )
```

time: 242 us -> 162 us (0.67)
  Pallas kernels: 0 us -> 156 us
  waiting for transfers between devices: 105 us -> 0 us
  blocking collectives: 53.3 us -> 0 us
  starting transfers between devices: 25.5 us -> 0 us
  matrix products: 17.5 us -> 0 us
  between operations: 13.6 us -> 0.01 us
  other arithmetic: 7.65 us -> 0 us
  local copies, waits for them, and re-layouts: 12.3 us -> 4.91 us
  loops' own time: 5.7 us -> 0 us
    pallas_call x0 -> x1, Pallas kernels: none -> 156 us  [shards(): pl.pallas_call(functools.partial(layer_kernel, chips), out_shape=jax.Shap...]
    all_gather x2 -> x0, waiting for transfers between devices: 105 us -> none  [the longest x1 60.4 us: sent_together(): lax.all_gather(both, axis, axis=dim, tiled=True)]
    all_to_all x3 -> x0, blocking collectives: 53.3 us -> none  [the longest x2 37.3 us: sum_at_owner(): lax.all_to_all(parts, axis, split_axis=0, concat_axis=0, tiled=True)]
    all_to_all x1 -> x0, starting transfers between devices: 25.5 us -> none  [sent_to_all(): return lax.all_to_all(copies, axis, split_axis=0, concat_axis=0, tiled=True)]
    dot_general x4 -> x0, matrix products: 17.5 us -> none  [the longest x1 11.3 us: shards(): jnp.dot(active, down_full, preferred_element_type=jnp.float32)]
    another operation x9 -> x0, loops' own time: 5.7 us -> none  [the longest x1 5.53 us: shards(): lax.scan(scan_block, carry_state, jnp.arange(row_count // block_span, dty...]
    dynamic_slice x8 -> x0, local copies, waits for them, and re-layouts: 4.69 us -> none  [shards(): lax.scan(scan_block, carry_state, jnp.arange(row_count // block_span, dty...]
    split x1 -> x0, local copies, waits for them, and re-layouts: 4.46 us -> none  [sent_together(): jnp.split(lax.all_gather(both, axis, axis=dim, tiled=True), ends, axis=al...]
  transfers between devices with their start and end apart: 3 -> 0, of which waited for: 2 -> 0; matrix products, arithmetic and copies ran while one was open for 10% -> 0% of each run, Pallas kernels for 0% -> 0%
where the time goes in v1:
time: 162 us; the launch traced here: 161 us
  Pallas kernels  156 us (96%)
  local copies, waits for them, and re-layouts  4.91 us (3%)
    pallas_call x1, Pallas kernels, shards(): pl.pallas_call(functools.partial(layer_kernel, chips), out_shape=jax.Shap...  156 us
    unnamed x2, local copies, waits for them, and re-layouts  3.62 us

profile of v1, /device:TPU:33, one launch (start us, length us, event | category | flops | bytes accessed | tf_op | source)
XLA Modules:
  0.0 161.3 jit_solution(1176461861147407452)
XLA Ops:
  0.0 1.3 pad.4.f_hbm
  1.3 1.9 %copy.12.wd_hbm = bf16[2048,64]{1,0:T(8,128)(2,1)} copy(bf16[2048,64]{0,1:T(8,128)(2,1)} %param.19) | data formatting | bytes 524288 | tf_op args[8]
  3.2 156.4 %layer.1 = bf16[64,2048]{1,0:T(8,128)(2,1)} custom-call(bf16[256,512]{1,0:T(8,128)(2,1)} %q_hbm.1, bf16[256,128]{1,0:T(8,128)(2,1)} %k_hbm.1, bf16[256,128]{1,0:T(8,128)(2,1)} %v_hbm.1, f32[8,256]{1,0:T(8,128)} %pad.4.f_hbm, bf16[64,2048]{1,0:T(8,128)(2,1)} %res_ref.1, f32[4,128]{1,0:T(4,128)} %bitcast.7, bf16[512,2048]{1,0:T(8,128)(2,1)} %wo_hbm.1, ...), custom_call_target="tpu_custom_call" | custom-call | tf_op jit(solution)/shard_map/layer/pallas_call | solution.py:451
  159.7 1.7 %copy.14 = bf16[64,2048]{1,0:T(8,128)(2,1)} copy(bf16[64,2048]{1,0:T(8,128)(2,1)} %layer.1) | data formatting | bytes 524288

commit v2 on v1

v2 whole, which is shorter than its diff:
```python
import functools

import jax
import jax.numpy as jnp
from jax import lax
from jax.experimental import pallas as pl
from jax.experimental.pallas import tpu as pltpu
from jax.sharding import PartitionSpec as P

HD = 128
ALPHA = 8.0**0.25
EPSILON = 1e-05
NEG_FILL = -1e30
LOG2E = 1.4426950408889634
MESH = pl.DeviceIdType.MESH
F32 = jnp.float32
BF16 = jnp.bfloat16

KV, GATE, UP, DOWN = (0, 1, 2, 3), (4,), (5, 6), (7, 8)


def dot_nt(a, b):
    return lax.dot_general(a, b, (((1,), (1,)), ((), ())), preferred_element_type=F32)


def dot_nn(a, b):
    return lax.dot_general(a, b, (((1,), (0,)), ((), ())), preferred_element_type=F32)


def layer_kernel(
    chips,
    q_hbm, k_hbm, v_hbm, f_hbm, res_ref, hgain_ref, wo_hbm, wu_hbm, wd_hbm, mgain_ref, cgain_ref,
    out_ref,
    q_s, kv, gate, wo_s, wu, wd, acc, m_s, l_s, heads, bp, b1, b2t, b2, mid, act,
    dp, d1, d2t, d2, d3t, d3, keep, low,
    ring_send, ring_recv, twin_send, twin_recv, local, bx_send, bx_recv, mx_send, mx_recv,
    dx_send, dx_recv,
):
    far = chips // 2
    grp, sp, tp = lax.axis_index("grp"), lax.axis_index("sp"), lax.axis_index("tp")
    z, core = sp // 2, sp % 2
    pair = grp % 2
    rows = q_s.shape[1]
    ffh = act.shape[1]
    right = (grp, ((z + 1) % chips) * 2 + core, tp)
    left = (grp, ((z + chips - 1) % chips) * 2 + core, tp)
    twin = (grp, z * 2 + 1 - core, tp)
    xa = tp + 1 - 2 * (tp % 2)
    xb = 3 - tp
    dev_a, dev_b = (grp, sp, xa), (grp, sp, xb)
    dev_y = (grp + 1 - 2 * pair, sp, tp)
    peers = (right, left, twin, dev_a, dev_b, dev_y)

    def remote(src, dst, ss, rs, dev):
        return pltpu.make_async_remote_copy(
            src_ref=src, dst_ref=dst, send_sem=ss, recv_sem=rs, device_id=dev, device_id_type=MESH
        )

    def when(cond, fn):
        if isinstance(cond, bool):
            if cond:
                fn()
        else:
            pl.when(cond)(fn)

    def both(a, b):
        return (a and b) if isinstance(a, bool) and isinstance(b, bool) else jnp.logical_and(a, b)

    def piece(st, slot):
        if st in KV:
            n = rows // 2
            return kv.at[slot, st // 2, pl.ds(st % 2 * n, n)]
        if st in GATE:
            return gate.at[slot]
        group, buf = (UP, wu) if st in UP else (DOWN, wd)
        n = buf.shape[1] // len(group)
        return buf.at[slot, pl.ds((st - group[0]) * n, n)]

    def ring_copy(st, way, slot, s):
        buf = piece(st, slot)
        return remote(buf, buf, ring_send.at[st, way], ring_recv.at[st, way, s], right if way == 0 else left)

    def twin_copy(st, way, slot, s):
        buf = piece(st, slot)
        return remote(buf, buf, twin_send.at[st, way], twin_recv.at[st, way, s], twin)

    def chip_at(way, s):
        return (z + chips - s) % chips if way == 0 else (z + s) % chips

    first_half = far - 2
    lower, top = z <= first_half, z == chips - 1

    def ring_begin(group, way):
        for st in group:
            ring_copy(st, way, sp, 1).start()

    def twin_begin(group):
        for st in group:
            twin_copy(st, 0, sp, 0).start()

    def ring_step(group, s):
        with jax.named_scope("ring%d" % group[0]):

            def one(st, way, last):
                slot = chip_at(way, s) * 2 + core
                ring_copy(st, way, slot, s).wait_recv()
                ring_copy(st, way, slot, s).wait_send()
                when(s < last, lambda: ring_copy(st, way, slot, s + 1).start())
                when(way == 0 or s > 1, lambda: twin_copy(st, way, slot, s).wait_send())
                twin_copy(st, way, slot, s).start()

            def both_ways():
                for st in group:
                    one(st, 0, far)
                    one(st, 1, far - 1)

            def one_way():
                for st in group:
                    one(st, 0, far)

            when(s < far, both_ways)
            when(s == far, one_way)

    def causal_step(group, s):
        def up(st):
            slot = chip_at(0, s) * 2 + core
            ring_copy(st, 0, slot, s).wait_recv()

            @pl.when(jnp.logical_not(top))
            def _():
                ring_copy(st, 0, slot, s).wait_send()
                when(s < far, lambda: ring_copy(st, 0, slot, s + 1).start())

            twin_copy(st, 0, slot, s).wait_send()
            twin_copy(st, 0, slot, s).start()

        def down(st):
            slot = chip_at(1, s) * 2 + core
            ring_copy(st, 1, slot, s).wait_recv()

            @pl.when(jnp.logical_or(lower, z + s > chips))
            def _():
                ring_copy(st, 1, slot, s).wait_send()

            when(s < far - 1, lambda: ring_copy(st, 1, slot, s + 1).start())

            @pl.when(z + s >= chips)
            def _():
                @pl.when(z + s > chips)
                def _():
                    twin_copy(st, 1, slot, s).wait_send()

                twin_copy(st, 1, slot, s).start()

        with jax.named_scope("kv"):

            @pl.when(z - s >= 0)
            def _():
                for st in group:
                    up(st)

            @pl.when(jnp.logical_and(s < far, jnp.logical_or(z + s <= first_half, z + s >= chips)))
            def _():
                for st in group:
                    down(st)

    def causal_wait(group, s):
        with jax.named_scope("kvtwin"):

            @pl.when(z - s >= 0)
            def _():
                for st in group:
                    twin_copy(st, 0, chip_at(0, s) * 2 + 1 - core, s).wait_recv()

            @pl.when(jnp.logical_and(s < far, z + s >= chips))
            def _():
                for st in group:
                    twin_copy(st, 1, chip_at(1, s) * 2 + 1 - core, s).wait_recv()

    def causal_end(group):
        for st in group:
            twin_copy(st, 0, sp, 0).wait_send()

        @pl.when(z < far)
        def _():
            for st in group:
                ring_copy(st, 0, sp, 1).wait_send()

        @pl.when(lower)
        def _():
            for st in group:
                ring_copy(st, 1, sp, 1).wait_send()

        @pl.when(z + far > chips)
        def _():
            for st in group:
                twin_copy(st, 1, sp, 1).wait_send()

    def twin_wait(group, s):
        with jax.named_scope("twin%d" % group[0]):
            for st in group:
                twin_copy(st, 0, chip_at(0, s) * 2 + 1 - core, s).wait_recv()

            def other():
                for st in group:
                    twin_copy(st, 1, chip_at(1, s) * 2 + 1 - core, s).wait_recv()

            when(both(s > 0, s < far), other)

    def ring_end(group):
        for st in group:
            twin_copy(st, 0, sp, 0).wait_send()
            twin_copy(st, 1, sp, 0).wait_send()

    loads = [
        pltpu.make_async_copy(k_hbm, kv.at[sp, 0], local.at[0]),
        pltpu.make_async_copy(v_hbm, kv.at[sp, 1], local.at[1]),
        pltpu.make_async_copy(f_hbm, gate.at[sp], local.at[2]),
        pltpu.make_async_copy(wu_hbm.at[:, pl.ds(pl.multiple_of(pair * ffh, ffh), ffh)], wu.at[sp], local.at[3]),
        pltpu.make_async_copy(wd_hbm.at[:, pl.ds(pl.multiple_of(pair * ffh, ffh), ffh)], wd.at[sp], local.at[4]),
        pltpu.make_async_copy(wo_hbm, wo_s, local.at[5]),
    ]
    loads += [pltpu.make_async_copy(q_hbm.at[:, pl.ds(h * HD, HD)], q_s.at[h], local.at[6 + h]) for h in range(4)]
    for c in loads:
        c.start()

    with jax.named_scope("entry"):
        barrier = pltpu.get_barrier_semaphore()
        for dev in peers:
            pl.semaphore_signal(barrier, inc=1, device_id=dev, device_id_type=MESH)
        pl.semaphore_wait(barrier, len(peers))
        for c in loads[:3]:
            c.wait()

        @pl.when(jnp.logical_not(top))
        def _():
            ring_begin(KV + GATE, 0)

        @pl.when(lower)
        def _():
            ring_begin(KV + GATE, 1)

        twin_begin(KV + GATE)
        loads[3].wait()

        @pl.when(jnp.logical_not(lower))
        def _():
            ring_begin(UP, 1)

        @pl.when(top)
        def _():
            ring_begin(UP, 0)

    gate_base = [None] * 4
    own_gate = gate[sp]
    for h in range(4):
        gate_base[h] = own_gate[h : h + 1, 0:1]

    def scores(h, src):
        s = dot_nt(q_s[h], kv[src, 0])
        bias = (gate_base[h] - gate[src][h : h + 1, :]) * LOG2E
        return s * (HD**-0.5 * LOG2E) + bias

    def spread(col):
        return jnp.broadcast_to(col, (rows, HD))

    for c in loads[6:]:
        c.wait()
    with jax.named_scope('diag'):
        causal = lax.broadcasted_iota(jnp.int32, (rows, rows), 1) <= lax.broadcasted_iota(jnp.int32, (rows, rows), 0)
        for h in range(4):
            s = jnp.where(causal, scores(h, sp), NEG_FILL)
            m = spread(jnp.max(s, axis=1, keepdims=True))
            p = jnp.exp2(s - jnp.concatenate([m] * (rows // HD), axis=1))
            m_s[h] = m
            l_s[h] = spread(jnp.sum(p, axis=1, keepdims=True))
            acc[h] = dot_nn(p.astype(BF16), kv[sp, 1])

    def attend(srcs):
        with jax.named_scope('attend'):
            attend_(srcs)

    def attend_(srcs):
        for h in range(4):
            ss = [scores(h, src) for src in srcs]
            top = functools.reduce(jnp.maximum, ss)
            m_old = m_s[h]
            m = jnp.maximum(m_old, spread(jnp.max(top, axis=1, keepdims=True)))
            wide = jnp.concatenate([m] * (rows // HD), axis=1)
            ps = [jnp.exp2(s - wide) for s in ss]
            fade = jnp.exp2(m_old - m)
            total = functools.reduce(jnp.add, ps)
            m_s[h] = m
            l_s[h] = l_s[h] * fade + spread(jnp.sum(total, axis=1, keepdims=True))
            out = dot_nn(ps[0].astype(BF16), kv[srcs[0], 1])
            for p, src in zip(ps[1:], srcs[1:]):
                out = out + dot_nn(p.astype(BF16), kv[src, 1])
            acc[h] = acc[h] * fade + out

    def attend_step(s):
        @pl.when(z - s >= 0)
        def _():
            c = chip_at(0, s) * 2
            attend([c, c + 1])

        @pl.when(jnp.logical_and(s < far, z + s >= chips))
        def _():
            c = chip_at(1, s) * 2
            attend([c, c + 1])

    def kv_step(s, carry):
        causal_step(KV + GATE, s)
        causal_wait(KV + GATE, s - 1)

        @pl.when(jnp.logical_and(s == 1, core == 1))
        def _():
            attend([sp - 1])

        @pl.when(s > 1)
        def _():
            attend_step(s - 1)

        return carry

    lax.fori_loop(1, far + 1, kv_step, 0)

    @pl.when(lower)
    def _():
        ring_begin(UP, 1)

    @pl.when(jnp.logical_not(top))
    def _():
        ring_begin(UP, 0)

    twin_begin(UP)
    causal_wait(KV + GATE, far)
    attend_step(far)
    causal_end(KV + GATE)

    loads[4].wait()
    cols = wd.shape[1]

    loads[5].wait()
    with jax.named_scope('headnorm'):
        for h in range(4):
            att = acc[h] / l_s[h]
            norm = lax.rsqrt(jnp.mean(att * att, axis=1, keepdims=True) + EPSILON)
            heads[:, h * HD : (h + 1) * HD] = (att * norm * hgain_ref[h : h + 1, :]).astype(BF16)
    half = bp.shape[3]
    own = bp.shape[2]
    with jax.named_scope('wout'):
        for j in range(4):
            w = half // 2
            part = dot_nn(heads[...], wo_s[:, j * w : (j + 1) * w]).astype(BF16)
            bp[j // 2, :, :, (j % 2) * w : (j % 2 + 1) * w] = part.reshape(4, own, w)

    far_a = 3 - xa
    first = (dev_a, dev_b)
    second = (dev_b, dev_a)
    first_x = (xa, xb)
    second_x = (xb, xa)

    def b1_copy(hf, j):
        src = bp.at[hf, first_x[hf] if j == 0 else far_a]
        return remote(src, b1.at[hf, j], bx_send.at[hf, j], bx_recv.at[hf, j], first[hf])

    def b2_copy(hf):
        return remote(b2t.at[hf], b2.at[hf], bx_send.at[hf, 2], bx_recv.at[hf, 2], second[hf])

    for hf in range(2):
        b1_copy(hf, 1).start()
    for hf in range(2):
        b1_copy(hf, 0).start()
    ring_step(UP, 1)
    with jax.named_scope('b1'):
        for hf in range(2):
            b1_copy(hf, 1).wait_recv()
            b2t[hf] = (bp[hf, second_x[hf]].astype(F32) + b1[hf, 1].astype(F32)).astype(BF16)
            b2_copy(hf).start()
    ring_step(UP, 2)
    sums = []
    with jax.named_scope('b1w'):
        for hf in range(2):
            b1_copy(hf, 0).wait_recv()
    ring_step(UP, 3)
    with jax.named_scope('b2'):
        for hf in range(2):
            b2_copy(hf).wait_recv()
            part = bp[hf, tp].astype(F32) + b1[hf, 0].astype(F32) + b2[hf].astype(F32)
            sums.append(ALPHA * res_ref[:, hf * half : (hf + 1) * half].astype(F32) + part)

    def layer_norm(parts, gain_ref):
        width = 2 * half
        mean = sum(jnp.sum(p, axis=1, keepdims=True) for p in parts) * (1.0 / width)
        parts = [p - mean for p in parts]
        var = sum(jnp.sum(p * p, axis=1, keepdims=True) for p in parts) * (1.0 / width)
        inv = lax.rsqrt(var + EPSILON)
        return [
            (p * inv * gain_ref[:, i * half : (i + 1) * half]).astype(BF16) for i, p in enumerate(parts)
        ]

    with jax.named_scope('ln1'):
        for hf, part in enumerate(layer_norm(sums, mgain_ref)):
            mid[hf, tp, pair] = part

    def my_copy(hf):
        return remote(mid.at[hf, tp, pair], mid.at[hf, tp, pair], mx_send.at[hf, 0], mx_recv.at[hf, 0], dev_y)

    def m1_copy(hf, j):
        ref = mid.at[hf, tp, pair if j == 0 else 1 - pair]
        return remote(ref, ref, mx_send.at[hf, 1 + j], mx_recv.at[hf, 1 + j], first[hf])

    def m2_copy(hf, j):
        ref = mid.at[hf, tp if j == 0 else first_x[hf]]
        return remote(ref, ref, mx_send.at[hf, 3 + j], mx_recv.at[hf, 3 + j], second[hf])

    for hf in range(2):
        my_copy(hf).start()
        m1_copy(hf, 0).start()
    ring_step(UP, 4)
    with jax.named_scope('my'):
        for hf in range(2):
            my_copy(hf).wait_recv()
            m1_copy(hf, 1).start()
            m2_copy(hf, 0).start()
    ring_step(UP, 5)
    ring_step(UP, 6)
    for way in range(2):
        ring_begin(DOWN, way)
    twin_begin(DOWN)
    with jax.named_scope('m1'):
        for hf in range(2):
            m1_copy(hf, 0).wait_recv()
            m1_copy(hf, 1).wait_recv()
            m2_copy(hf, 1).start()
    ring_step(UP, 7)
    ring_step(UP, 8)
    for s in range(far + 1):
        twin_wait(UP, s)
    ring_step(DOWN, 1)
    ring_step(DOWN, 2)
    with jax.named_scope('m2'):
        for hf in range(2):
            m2_copy(hf, 0).wait_recv()
            m2_copy(hf, 1).wait_recv()
    ring_end(UP)

    toks = act.shape[0]
    tile = 256

    def up_tile(j, carry):
        cs = pl.ds(pl.multiple_of(j * tile, tile), tile)
        total = None
        for hf in range(2):
            blocks = wu.shape[0] // 2
            w = wu[hf * blocks : (hf + 1) * blocks, :, cs].reshape(half, tile)
            part = dot_nn(mid[hf].reshape(toks, half), w)
            total = part if total is None else total + part
        pos = jnp.maximum(total, 0.0)
        act[:, cs] = (pos * pos).astype(BF16)
        return carry

    with jax.named_scope('up'):
        lax.fori_loop(0, ffh // tile // 2, up_tile, 0)
    ring_step(DOWN, 3)
    with jax.named_scope('up'):
        lax.fori_loop(ffh // tile // 2, ffh // tile, up_tile, 0)
    early = 3

    wide = 2 * cols

    def chunk_chip(t, hf):
        return jnp.where(t == far, z, chip_at(0, t)) if hf == 0 else jnp.where(t == far, chip_at(0, t), chip_at(1, t))

    def d1_copy(t, hf, j):
        src = dp.at[t - 1, hf, first_x[hf] if j == 0 else far_a]
        return remote(src, d1.at[t - 1, hf, j], dx_send.at[t - 1, hf, j], dx_recv.at[t - 1, hf, j], first[hf])

    def d2_copy(t, hf):
        return remote(
            d2t.at[t - 1, hf], d2.at[t - 1, hf], dx_send.at[t - 1, hf, 2], dx_recv.at[t - 1, hf, 2], second[hf]
        )

    def d3_copy(t, hf):
        return remote(
            d3t.at[t - 1, hf], d3.at[t - 1, hf], dx_send.at[t - 1, hf, 3], dx_recv.at[t - 1, hf, 3], dev_y
        )

    def down_step(i, carry):
        @pl.when(jnp.logical_and(i > early, i <= far))
        def _():
            ring_step(DOWN, i)

        @pl.when(jnp.logical_and(i >= 2, i <= far + 1))
        def _():
            t = i - 1
            twin_wait(DOWN, t)

            @pl.when(t == far)
            def _():
                twin_wait(DOWN, 0)

            with jax.named_scope('down'):
                w = jnp.concatenate(
                    [wd[pl.ds(chunk_chip(t, hf) * 2, 2)].reshape(wide, ffh) for hf in range(2)], axis=0
                )
                part = dot_nt(act[...], w).astype(BF16)
                for hf in range(2):
                    dp[t - 1, hf] = part[:, hf * wide : (hf + 1) * wide].reshape(4, 2, own, wide)
                    d1_copy(t, hf, 1).start()
                    d1_copy(t, hf, 0).start()

        @pl.when(jnp.logical_and(i >= 3, i <= far + 2))
        def _():
            with jax.named_scope('d1'):
                t = i - 2
                for hf in range(2):
                    d1_copy(t, hf, 1).wait_recv()
                    d2t[t - 1, hf] = (
                        dp[t - 1, hf, second_x[hf]].astype(F32) + d1[t - 1, hf, 1].astype(F32)
                    ).astype(BF16)
                    d2_copy(t, hf).start()

        @pl.when(jnp.logical_and(i >= 4, i <= far + 3))
        def _():
            with jax.named_scope('d2'):
                t = i - 3
                for hf in range(2):
                    d1_copy(t, hf, 0).wait_recv()
                    d2_copy(t, hf).wait_recv()

                    def whole(y):
                        return (
                            dp[t - 1, hf, tp, y].astype(F32)
                            + d1[t - 1, hf, 0, y].astype(F32)
                            + d2[t - 1, hf, y].astype(F32)
                        )

                    d3t[t - 1, hf] = whole(1 - pair).astype(BF16)
                    d3_copy(t, hf).start()
                    keep[t - 1, hf] = whole(pair)

        @pl.when(i >= 5)
        def _():
            with jax.named_scope('d3'):
                t = i - 4
                for hf in range(2):
                    d3_copy(t, hf).wait_recv()
                    cs = pl.ds(pl.multiple_of(chunk_chip(t, hf) * wide, wide), wide)
                    low[:, cs] = keep[t - 1, hf] + d3[t - 1, hf].astype(F32)
                    for j in range(2):
                        d1_copy(t, hf, j).wait_send()
                    d2_copy(t, hf).wait_send()
                    d3_copy(t, hf).wait_send()

        return carry

    lax.fori_loop(1, far + 5, down_step, 0)
    ring_end(DOWN)

    with jax.named_scope('ln2'):
        sums = [
            ALPHA * mid[hf, tp, pair].astype(F32) + low[:, hf * half : (hf + 1) * half] for hf in range(2)
        ]
        for hf, part in enumerate(layer_norm(sums, cgain_ref)):
            out_ref[:, hf * half : (hf + 1) * half] = part

    for hf in range(2):
        for j in range(2):
            b1_copy(hf, j).wait_send()
            m1_copy(hf, j).wait_send()
            m2_copy(hf, j).wait_send()
        b2_copy(hf).wait_send()
        my_copy(hf).wait_send()


def solution(mesh):
    spn, tpn = mesh.shape["sp"], mesh.shape["tp"]
    chips = spn // 2
    assert spn % 4 == 0 and tpn == 4 and mesh.shape["grp"] % 2 == 0

    def shards(res, q, k, v, f, hgain, wo, wu, wd, mgain, cgain):
        rows = q.shape[0]
        own, width = res.shape
        half = width // 2
        up_rows, ff = wu.shape
        ffh = ff // 2
        cols = wd.shape[1]
        wide = 2 * cols
        far = chips // 2
        toks = 2 * 4 * own
        any_spec = pl.BlockSpec(memory_space=pl.ANY)
        vmem = pl.BlockSpec(memory_space=pltpu.VMEM)
        dma = pltpu.SemaphoreType.DMA
        return pl.pallas_call(
            functools.partial(layer_kernel, chips),
            out_shape=jax.ShapeDtypeStruct((own, width), BF16),
            in_specs=[any_spec, any_spec, any_spec, any_spec, vmem, vmem, any_spec, any_spec, any_spec, vmem, vmem],
            out_specs=vmem,
            scratch_shapes=[
                pltpu.VMEM((4, rows, HD), BF16),
                pltpu.VMEM((spn, 2, rows, HD), BF16),
                pltpu.VMEM((spn, 4, rows), F32),
                pltpu.VMEM(wo.shape, BF16),
                pltpu.VMEM((spn, up_rows, ffh), BF16),
                pltpu.VMEM((spn, cols, ffh), BF16),
                pltpu.VMEM((4, rows, HD), F32),
                pltpu.VMEM((4, rows, HD), F32),
                pltpu.VMEM((4, rows, HD), F32),
                pltpu.VMEM((rows, 4 * HD), BF16),
                pltpu.VMEM((2, 4, own, half), BF16),
                pltpu.VMEM((2, 2, own, half), BF16),
                pltpu.VMEM((2, own, half), BF16),
                pltpu.VMEM((2, own, half), BF16),
                pltpu.VMEM((2, 4, 2, own, half), BF16),
                pltpu.VMEM((toks, ffh), BF16),
                pltpu.VMEM((far, 2, 4, 2, own, wide), BF16),
                pltpu.VMEM((far, 2, 2, 2, own, wide), BF16),
                pltpu.VMEM((far, 2, 2, own, wide), BF16),
                pltpu.VMEM((far, 2, 2, own, wide), BF16),
                pltpu.VMEM((far, 2, own, wide), BF16),
                pltpu.VMEM((far, 2, own, wide), BF16),
                pltpu.VMEM((far, 2, own, wide), F32),
                pltpu.VMEM((own, width), F32),
                dma((9, 2)),
                dma((9, 2, far + 1)),
                dma((9, 2)),
                dma((9, 2, far + 1)),
                dma((10,)),
                dma((2, 3)),
                dma((2, 3)),
                dma((2, 5)),
                dma((2, 5)),
                dma((far, 2, 4)),
                dma((far, 2, 4)),
            ],
            compiler_params=pltpu.CompilerParams(
                collective_id=0, has_side_effects=True, vmem_limit_bytes=56 * 1024 * 1024
            ),
            name="layer",
        )(q, k, v, f.T, res, hgain.reshape(4, HD), wo, wu, wd.T, mgain.reshape(1, width), cgain.reshape(1, width))

    def body(residual_in, query_rows, key_rows, value_rows, forget_cumsum, head_gain, w_out, w_up, w_down, mixer_gain, channel_gain):
        return shards(
            residual_in, query_rows, key_rows, value_rows, forget_cumsum, head_gain, w_out, w_up, w_down,
            mixer_gain, channel_gain,
        )

    placed = (
        P(("grp", "sp", "tp"), None),
        P(("grp", "sp"), "tp"),
        P(("grp", "sp"), "tp"),
        P(("grp", "sp"), "tp"),
        P(("grp", "sp"), "tp"),
        P("tp"),
        P("tp", None),
        P("sp", "tp"),
        P("tp", "sp"),
        P(),
        P(),
    )
    return jax.shard_map(
        body, mesh=mesh, in_specs=placed, out_specs=P(("grp", "sp", "tp"), None), check_vma=False
    )
```

time: 162 us -> 143 us (0.88)
  Pallas kernels: 156 us -> 141 us
  local copies, waits for them, and re-layouts: 4.91 us -> 1.67 us
    pallas_call x1, Pallas kernels: 156 us -> 141 us  [shards(): pl.pallas_call(functools.partial(layer_kernel, chips), out_shape=jax.Shap...]
    unnamed x2 -> x1, local copies, waits for them, and re-layouts: 3.62 us -> 1.67 us
where the time goes in v2:
time: 143 us; the launch traced here: 142 us
  Pallas kernels  141 us (99%)
  local copies, waits for them, and re-layouts  1.67 us (1%)
    pallas_call x1, Pallas kernels, shards(): pl.pallas_call(functools.partial(layer_kernel, chips), out_shape=jax.Shap...  141 us

profile of v2, /device:TPU:33, one launch (start us, length us, event | category | flops | bytes accessed | tf_op | source)
XLA Modules:
  0.0 142.3 jit_solution(6644431724704200714)
XLA Ops:
  0.0 140.6 %layer.1 = bf16[64,2048]{1,0:T(8,128)(2,1)} custom-call(bf16[256,512]{1,0:T(8,128)(2,1)} %q_hbm.1, bf16[256,128]{1,0:T(8,128)(2,1)} %k_hbm.1, bf16[256,128]{1,0:T(8,128)(2,1)} %v_hbm.1, f32[4,256]{1,0:T(4,128)} %bitcast.8, bf16[64,2048]{1,0:T(8,128)(2,1)} %res_ref.1, f32[4,128]{1,0:T(4,128)} %bitcast.9, bf16[512,2048]{1,0:T(8,128)(2,1)} %wo_hbm.1, ...), custom_call_target="tpu_custom_call" | custom-call | tf_op jit(solution)/shard_map/layer/pallas_call | solution.py:595
  140.6 1.7 %copy.13 = bf16[64,2048]{1,0:T(8,128)(2,1)} copy(bf16[64,2048]{1,0:T(8,128)(2,1)} %layer.1) | data formatting | bytes 524288
